TPU v7x, 128 devices: a whole 4x4x4 slice. The times are simulated.
128 devices in a mesh: sp: 16 (over z, y), dp: 8 (over x, core).
Axes of the slice: x: 4, y: 4, z: 4, core: 2. Of those that a mesh axis runs over, the one named last changes fastest.
Arguments:
- tokens: bfloat16 [8, 5120, 2048], P('dp', 'sp'), may hold values from -6 to 6
- w_query: bfloat16 [2048, 1024], P('dp', 'sp'), may hold values from -0.125 to 0.125
- w_key: bfloat16 [2048, 1024], P('dp', 'sp'), may hold values from -0.125 to 0.125
- w_value: bfloat16 [2048, 1024], P('dp', 'sp'), may hold values from -0.125 to 0.125
- w_output: bfloat16 [1024, 2048], P('sp', 'dp'), may hold values from -0.1875 to 0.1875
- qk_gain: float32 [2, 64], replicated, may hold values from 0.4 to 7
- decay_sums: float32 [8, 16, 5120], P('dp', 'sp'), may hold values from -1024 to 0, as said below
Outputs:
- layer_out: bfloat16 [8, 5120, 2048], P('dp', 'sp')
Inputs may be any that keep to these rules, and one draw needn't show every extreme that they name: `decay_sums`: each row is non-increasing along positions.
All inputs are finite; a program needn't handle non-finite values.
Results may differ from a plain program's by a relative error of at most 0.0075.
The roundings to bfloat16 on the way count: a program that leaves them out, or rounds other values in their place, can miss the bound.
Values may be sent and summed in bfloat16 or wider, within the bound.
No kernel may reach another device: no remote copies, remote signals or barrier semaphores. Data moves between devices by JAX's collectives and lax.ppermute only.
A program may use at most 128 MiB of HBM per device.

v0:
```python
import jax
import jax.numpy as jnp
from jax import lax
from jax.sharding import Mesh
from jax.sharding import PartitionSpec as P

DP = ("dp_0", "dp_1")
SP = ("sp_0", "sp_1")


def piece_ends(length, count):
    lap = length // count
    if lap >= 8:
        lap -= lap % 8
    return [lap * k for k in range(1, count)]


def all_blocks(value, axes, order):
    pieces = value
    for k in order:
        pieces = lax.all_gather(pieces, axes[k])
    done = order[::-1]
    back = [done.index(k) for k in range(len(axes))]
    pieces = pieces.transpose(*back, *range(len(axes), pieces.ndim))
    return pieces.reshape(-1, *value.shape)


def in_order(pieces, dim):
    lengths = list(pieces.shape[1:])
    lengths[dim] *= pieces.shape[0]
    return jnp.moveaxis(pieces, 0, dim).reshape(lengths)


def spread_gather(value, axes, dim):
    split_at = max(range(max(1, value.ndim - 1)), key=lambda d: value.shape[d])
    count, outs = (len(axes), [])
    for leading, section in enumerate(
        jnp.split(value, piece_ends(value.shape[split_at], count), axis=split_at)
    ):
        if section.size:
            order = [(leading - k) % count for k in range(count)]
            outs.append(all_blocks(section, axes, order))
    return in_order(jnp.concatenate(outs, axis=split_at + 1), dim)


def normalize(values):
    values = values.astype(jnp.float32)
    return values * lax.rsqrt(jnp.mean(values * values, axis=-1, keepdims=True) + 1e-06)


def attend(query_unit, key_unit, value_rows, decay_rows):
    length = query_unit.shape[0]
    groups = query_unit.shape[1]
    width = query_unit.shape[2]
    block = min(512, length)

    def one_block(index):
        start = index * block
        query_block = lax.dynamic_slice_in_dim(query_unit, start, block, 0)
        decay_block = lax.dynamic_slice_in_dim(decay_rows, start, block, 1)
        query_place = start + jnp.arange(block, dtype=jnp.int32)

        def fill(column, buffer):
            key_start = column * block
            key_block = lax.dynamic_slice_in_dim(key_unit, key_start, block, 0)
            decay_keys = lax.dynamic_slice_in_dim(decay_rows, key_start, block, 1)
            scores = jnp.einsum(
                "qhd,khd->hqk", query_block, key_block, preferred_element_type=jnp.float32
            )
            scores = scores + decay_block[:, :, None] - decay_keys[:, None, :]
            key_place = key_start + jnp.arange(block, dtype=jnp.int32)
            scores = jnp.where(
                key_place[None, None, :] <= query_place[None, :, None], scores, -jnp.inf
            )
            return lax.dynamic_update_slice_in_dim(buffer, scores, key_start, 2)

        empty = jnp.full((groups, block, length), -jnp.inf, jnp.float32)
        scores = lax.fori_loop(0, index + 1, fill, empty)
        peak = jnp.max(scores, axis=-1, keepdims=True)
        weights = jnp.exp(scores - peak)
        probs = (weights / jnp.sum(weights, axis=-1, keepdims=True)).astype(jnp.bfloat16)

        def gather_values(column, running):
            key_start = column * block
            prob_block = lax.dynamic_slice_in_dim(probs, key_start, block, 2)
            value_block = lax.dynamic_slice_in_dim(value_rows, key_start, block, 0)
            return running + jnp.einsum(
                "hqk,khd->qhd", prob_block, value_block, preferred_element_type=jnp.float32
            )

        zeros = jnp.zeros((block, groups, width), jnp.float32)
        return lax.fori_loop(0, index + 1, gather_values, zeros)

    blocks = lax.map(one_block, jnp.arange(length // block, dtype=jnp.int32))
    return blocks.reshape(length, groups, width)


def on_device(tokens, w_query, w_key, w_value, w_output, qk_gain, decay_sums):
    own_rows = tokens[0]
    decay_rows = decay_sums[0]
    head_group = decay_rows.shape[0]
    head_dim = qk_gain.shape[1]
    stacked = jnp.stack((w_query, w_key, w_value))
    columns, out_columns = (spread_gather(stacked, DP, 1), spread_gather(w_output, DP, 1))
    whole = lax.all_gather(own_rows, SP, axis=0, tiled=True)
    triple = jnp.einsum("td,kdc->ktc", whole, columns, preferred_element_type=jnp.float32).astype(
        jnp.bfloat16
    )
    length = triple.shape[1]
    grouped = triple.reshape(3, length, head_group, head_dim)
    query_unit = (normalize(grouped[0]) * qk_gain[0] * head_dim ** (-0.5)).astype(jnp.bfloat16)
    key_unit = (normalize(grouped[1]) * qk_gain[1]).astype(jnp.bfloat16)
    attended = attend(query_unit, key_unit, grouped[2], decay_rows)
    head_out = normalize(attended).astype(jnp.bfloat16).reshape(length, head_group * head_dim)
    merged = lax.all_to_all(head_out, SP, split_axis=0, concat_axis=1, tiled=True)
    result = jnp.dot(merged, spread_gather(out_columns, SP, 0), preferred_element_type=jnp.float32)
    return result.astype(jnp.bfloat16)[None]


def solution(mesh):
    torus = Mesh(mesh.devices.reshape(4, 4, 4, 2), ("sp_0", "sp_1", "dp_0", "dp_1"))
    in_specs = (P(DP, SP, None), P(DP, SP), P(DP, SP), P(DP, SP), P(SP, DP), P(), P(DP, SP, None))
    out_specs = P(DP, SP, None)
    return jax.shard_map(
        on_device, mesh=torus, in_specs=in_specs, out_specs=out_specs, check_vma=False
    )
```

profile of v0, /device:TPU:0, one launch (start us, length us, event | category | flops | bytes accessed | tf_op | source)
XLA Modules:
  0.0 617.3 jit_solution(8248347875593230595)
XLA Ops:
  8.0 12.3 %all-gather.5 = bf16[128,256]{1,0:T(8,128)(2,1)S(1)} all-gather(bf16[32,256]{1,0:T(8,128)(2,1)S(1)} %get-tuple-element.211), channel_id=7, replica_groups=mesh['sp_0'=4,'sp_1'=4,'dp_0'=4,'dp_1'=2] {'dp_0'}, dimensions={0}, use_global_device_ids=true | all-gather | bytes 81920 | tf_op jit(solution)/shard_map/all_gather | solution.py:21
  24.1 12.0 %all-gather.8 = bf16[8,32,256]{2,1,0:T(8,128)(2,1)S(1)} all-gather(bf16[2,32,256]{2,1,0:T(8,128)(2,1)S(1)} %bitcast.143), channel_id=10, replica_groups=mesh['sp_0'=4,'sp_1'=4,'dp_0'=4,'dp_1'=2] {'dp_0'}, dimensions={0}, use_global_device_ids=true | all-gather | bytes 163840 | tf_op jit(solution)/shard_map/all_gather | solution.py:21
  36.3 16.9 %all_gather.93 = bf16[4,32,2048]{2,1,0:T(8,128)(2,1)} all-gather(bf16[1,32,2048]{2,1,0:T(8,128)(2,1)S(1)} %all_gather.92), channel_id=1, replica_groups=mesh['sp_0'=4,'sp_1'=4,'dp_0'=4,'dp_1'=2] {'sp_0'}, dimensions={0}, use_global_device_ids=true | all-gather | bytes 655360 | tf_op jit(solution)/shard_map/all_gather | solution.py:21
  53.5 16.2 %all_gather.97 = bf16[4,32,2048]{2,1,0:T(8,128)(2,1)} all-gather(bf16[1,32,2048]{2,1,0:T(8,128)(2,1)S(1)} %all_gather.96), channel_id=1, replica_groups=mesh['sp_0'=4,'sp_1'=4,'dp_0'=4,'dp_1'=2] {'sp_1'}, dimensions={0}, use_global_device_ids=true | all-gather | bytes 655360 | tf_op jit(solution)/shard_map/all_gather | solution.py:21
  69.8 12.1 %all-gather = bf16[12,128,64]{1,2,0:T(8,128)(2,1)S(1)} all-gather(bf16[3,128,64]{1,2,0:T(8,128)(2,1)S(1)} %get-tuple-element.209), channel_id=2, replica_groups=mesh['sp_0'=4,'sp_1'=4,'dp_0'=4,'dp_1'=2] {'dp_0'}, dimensions={0}, use_global_device_ids=true | all-gather | bytes 245760 | tf_op jit(solution)/shard_map/all_gather | solution.py:21
  85.9 12.5 %all-gather.3 = bf16[8,3,128,64]{2,3,1,0:T(8,128)(2,1)S(1)} all-gather(bf16[2,3,128,64]{2,3,1,0:T(8,128)(2,1)S(1)} %bitcast.140), channel_id=5, replica_groups=mesh['sp_0'=4,'sp_1'=4,'dp_0'=4,'dp_1'=2] {'dp_0'}, dimensions={0}, use_global_device_ids=true | all-gather | bytes 491520 | tf_op jit(solution)/shard_map/all_gather | solution.py:21
  98.6 51.4 %all-gather.15.cloned.1.call-done = bf16[1,5120,2048]{2,1,0:T(8,128)(2,1)} async-done(((bf16[1,320,2048]{2,1,0:T(8,128)(2,1)}), bf16[1,5120,2048]{2,1,0:T(8,128)(2,1)}) %all-gather.15.cloned.1.call-update) | async-done | bytes 20971536 | tf_op jit(solution)/shard_map/all_gather | solution.py:105
  150.0 11.5 %fusion.23 = bf16[3,5120,64]{1,2,0:T(8,128)(2,1)S(1)} fusion(bf16[3,2048,64]{1,2,0:T(8,128)(2,1)S(1)} %bitcast.136, bf16[1,5120,2048]{2,1,0:T(8,128)(2,1)} %all-gather.15.cloned.1.call-done), kind=kOutput, calls=%fused_computation.30 | convolution fusion | flops 4027514880 | bytes 23724032 | tf_op jit(solution)/shard_map/td,kdc->ktc/dot_general | solution.py:106
  162.3 418.4 %while.33 = (s32[]{:T(128)}, f32[10,512,1,64]{1,3,2,0:T(8,128)S(1)}, s32[10]{0:T(128)S(1)}, bf16[5120,1,64]{0,2,1:T(8,128)(2,1)S(1)}, f32[1,5120]{1,0:T(1,128)},...) while((s32[]{:T(128)}, ...), condition=%wide.region_9.10_spmd, body=%wide.region_2.9_spmd.sunk | while | flops 83918864 | bytes 91718440 | solution.py:94
  177.2 5.6 fusion.60
  206.3 5.7 fusion.60
  227.9 6.0 while.34
  238.6 5.6 fusion.60
  261.4 8.1 %while.34 = (s32[]{:T(128)}, f32[1,512,5120]{1,2,0:T(8,128)}, s32[]{:T(128)}, bf16[5120,1,64]{0,2,1:T(8,128)(2,1)S(1)}, bf16[512,1,64]{0,2,1:T(8,128)(2,1)S(1)},...) while((s32[]{:T(128)}, f32[1,512,5120]{1,2,0:T(8,128)}, ...), condition=%wide.region_4.4_spmd.clone, body=%wide.region_3.3_spmd.clone.sunk | while | flops 34604036 | bytes 1197231 | solution.py:78
  274.2 5.6 fusion.60
  298.3 10.1 %while.34 = (s32[]{:T(128)}, f32[1,512,5120]{1,2,0:T(8,128)}, s32[]{:T(128)}, bf16[5120,1,64]{0,2,1:T(8,128)(2,1)S(1)}, bf16[512,1,64]{0,2,1:T(8,128)(2,1)S(1)},...) while((s32[]{:T(128)}, f32[1,512,5120]{1,2,0:T(8,128)}, ...), condition=%wide.region_4.4_spmd.clone, body=%wide.region_3.3_spmd.clone.sunk | while | flops 34604036 | bytes 1197231 | solution.py:78
  313.0 5.6 fusion.60
  323.9 6.4 %while.35 = (s32[]{:T(128)}, f32[512,1,64]{0,2,1:T(8,128)S(1)}, s32[]{:T(128)}, bf16[5120,1,64]{0,2,1:T(8,128)(2,1)S(1)}, bf16[1,512,5120]{1,2,0:T(8,128)(2,1)},...) while((s32[]{:T(128)}, f32[512,1,64]{0,2,1:T(8,128)S(1)}, s32[]{:T(128)}, ...), condition=%wide.region_8.8_spmd, body=%wide.region_7.7_spmd.sunk | while | flops 33587204 | bytes 853131 | solution.py:92
  338.4 12.1 %while.34 = (s32[]{:T(128)}, f32[1,512,5120]{1,2,0:T(8,128)}, s32[]{:T(128)}, bf16[5120,1,64]{0,2,1:T(8,128)(2,1)S(1)}, bf16[512,1,64]{0,2,1:T(8,128)(2,1)S(1)},...) while((s32[]{:T(128)}, f32[1,512,5120]{1,2,0:T(8,128)}, ...), condition=%wide.region_4.4_spmd.clone, body=%wide.region_3.3_spmd.clone.sunk | while | flops 34604036 | bytes 1197231 | solution.py:78
  355.2 5.6 fusion.60
  366.0 7.7 %while.35 = (s32[]{:T(128)}, f32[512,1,64]{0,2,1:T(8,128)S(1)}, s32[]{:T(128)}, bf16[5120,1,64]{0,2,1:T(8,128)(2,1)S(1)}, bf16[1,512,5120]{1,2,0:T(8,128)(2,1)},...) while((s32[]{:T(128)}, f32[512,1,64]{0,2,1:T(8,128)S(1)}, s32[]{:T(128)}, ...), condition=%wide.region_8.8_spmd, body=%wide.region_7.7_spmd.sunk | while | flops 33587204 | bytes 853131 | solution.py:92
  381.8 14.1 %while.34 = (s32[]{:T(128)}, f32[1,512,5120]{1,2,0:T(8,128)}, s32[]{:T(128)}, bf16[5120,1,64]{0,2,1:T(8,128)(2,1)S(1)}, bf16[512,1,64]{0,2,1:T(8,128)(2,1)S(1)},...) while((s32[]{:T(128)}, f32[1,512,5120]{1,2,0:T(8,128)}, ...), condition=%wide.region_4.4_spmd.clone, body=%wide.region_3.3_spmd.clone.sunk | while | flops 34604036 | bytes 1197231 | solution.py:78
  400.7 5.6 fusion.60
  411.5 9.0 %while.35 = (s32[]{:T(128)}, f32[512,1,64]{0,2,1:T(8,128)S(1)}, s32[]{:T(128)}, bf16[5120,1,64]{0,2,1:T(8,128)(2,1)S(1)}, bf16[1,512,5120]{1,2,0:T(8,128)(2,1)},...) while((s32[]{:T(128)}, f32[512,1,64]{0,2,1:T(8,128)S(1)}, s32[]{:T(128)}, ...), condition=%wide.region_8.8_spmd, body=%wide.region_7.7_spmd.sunk | while | flops 33587204 | bytes 853131 | solution.py:92
  428.6 16.2 %while.34 = (s32[]{:T(128)}, f32[1,512,5120]{1,2,0:T(8,128)}, s32[]{:T(128)}, bf16[5120,1,64]{0,2,1:T(8,128)(2,1)S(1)}, bf16[512,1,64]{0,2,1:T(8,128)(2,1)S(1)},...) while((s32[]{:T(128)}, f32[1,512,5120]{1,2,0:T(8,128)}, ...), condition=%wide.region_4.4_spmd.clone, body=%wide.region_3.3_spmd.clone.sunk | while | flops 34604036 | bytes 1197231 | solution.py:78
  449.4 5.6 fusion.60
  460.3 10.3 %while.35 = (s32[]{:T(128)}, f32[512,1,64]{0,2,1:T(8,128)S(1)}, s32[]{:T(128)}, bf16[5120,1,64]{0,2,1:T(8,128)(2,1)S(1)}, bf16[1,512,5120]{1,2,0:T(8,128)(2,1)},...) while((s32[]{:T(128)}, f32[512,1,64]{0,2,1:T(8,128)S(1)}, s32[]{:T(128)}, ...), condition=%wide.region_8.8_spmd, body=%wide.region_7.7_spmd.sunk | while | flops 33587204 | bytes 853131 | solution.py:92
  478.6 18.2 %while.34 = (s32[]{:T(128)}, f32[1,512,5120]{1,2,0:T(8,128)}, s32[]{:T(128)}, bf16[5120,1,64]{0,2,1:T(8,128)(2,1)S(1)}, bf16[512,1,64]{0,2,1:T(8,128)(2,1)S(1)},...) while((s32[]{:T(128)}, f32[1,512,5120]{1,2,0:T(8,128)}, ...), condition=%wide.region_4.4_spmd.clone, body=%wide.region_3.3_spmd.clone.sunk | while | flops 34604036 | bytes 1197231 | solution.py:78
  512.4 11.6 %while.35 = (s32[]{:T(128)}, f32[512,1,64]{0,2,1:T(8,128)S(1)}, s32[]{:T(128)}, bf16[5120,1,64]{0,2,1:T(8,128)(2,1)S(1)}, bf16[1,512,5120]{1,2,0:T(8,128)(2,1)},...) while((s32[]{:T(128)}, f32[512,1,64]{0,2,1:T(8,128)S(1)}, s32[]{:T(128)}, ...), condition=%wide.region_8.8_spmd, body=%wide.region_7.7_spmd.sunk | while | flops 33587204 | bytes 853131 | solution.py:92
  532.1 20.2 %while.34 = (s32[]{:T(128)}, f32[1,512,5120]{1,2,0:T(8,128)}, s32[]{:T(128)}, bf16[5120,1,64]{0,2,1:T(8,128)(2,1)S(1)}, bf16[512,1,64]{0,2,1:T(8,128)(2,1)S(1)},...) while((s32[]{:T(128)}, f32[1,512,5120]{1,2,0:T(8,128)}, ...), condition=%wide.region_4.4_spmd.clone, body=%wide.region_3.3_spmd.clone.sunk | while | flops 34604036 | bytes 1197231 | solution.py:78
  567.8 12.9 %while.35 = (s32[]{:T(128)}, f32[512,1,64]{0,2,1:T(8,128)S(1)}, s32[]{:T(128)}, bf16[5120,1,64]{0,2,1:T(8,128)(2,1)S(1)}, bf16[1,512,5120]{1,2,0:T(8,128)(2,1)},...) while((s32[]{:T(128)}, f32[512,1,64]{0,2,1:T(8,128)S(1)}, s32[]{:T(128)}, ...), condition=%wide.region_8.8_spmd, body=%wide.region_7.7_spmd.sunk | while | flops 33587204 | bytes 853131 | solution.py:92
  593.8 12.8 %all-to-all-done = bf16[16,320,64]{1,2,0:T(8,128)(2,1)S(1)} async-done(((bf16[16,320,64]{1,2,0:T(8,128)(2,1)}), bf16[16,320,64]{1,2,0:T(8,128)(2,1)S(1)}, u32[]{:S(2)}, u32[]{:S(2)}) %all-to-all-start) | async-done | bytes 655392 | tf_op jit(solution)/shard_map/all_to_all | solution.py:115
  (377 shorter events, 404.5 us)
Async XLA Ops:
  6.5 143.5 %all-gather.15.cloned.1.call-start = ((), (), s32[]{:S(2)}) async-start(), calls=%async_computation.1 | async-start | bytes 22282240 | tf_op jit(solution)/shard_map/all_gather | solution.py:105
  7.3 584.8 %all-gather.17.cloned.1.call-start = ((), (), s32[]{:S(2)}) async-start(), calls=%async_computation.2 | async-start | bytes 2621440 | tf_op jit(solution)/shard_map/all_gather | solution.py:21
  36.1 33.6 %copy-start.1 = (bf16[256,64]{0,1:T(8,128)(2,1)S(1)}, bf16[256,64]{0,1:T(8,128)(2,1)}, u32[]{:S(2)}) copy-start(bf16[256,64]{0,1:T(8,128)(2,1)} %param.16) | copy-start | bytes 98308
  36.1 33.6 %copy-start.2 = (bf16[256,64]{0,1:T(8,128)(2,1)S(1)}, bf16[256,64]{0,1:T(8,128)(2,1)}, u32[]{:S(2)}) copy-start(bf16[256,64]{0,1:T(8,128)(2,1)} %param.15) | copy-start | bytes 98308
  36.1 33.6 %copy-start.3 = (bf16[256,64]{0,1:T(8,128)(2,1)S(1)}, bf16[256,64]{0,1:T(8,128)(2,1)}, u32[]{:S(2)}) copy-start(bf16[256,64]{0,1:T(8,128)(2,1)} %param.14) | copy-start | bytes 98308
  53.3 540.5 %all-gather.19.cloned.1.call-start = ((), (), s32[]{:S(2)}) async-start(), calls=%async_computation.3 | async-start | bytes 2621440 | tf_op jit(solution)/shard_map/all_gather | solution.py:21
  84.0 14.6 %copy-start.4 = (f32[2,64]{1,0:T(2,128)S(1)}, f32[2,64]{1,0:T(2,128)}, u32[]{:S(2)}) copy-start(f32[2,64]{1,0:T(2,128)} %param.18) | copy-start | bytes 1540
  177.2 7.0 %copy-start = (f32[1,512,5120]{1,2,0:T(8,128)S(1)}, f32[1,512,5120]{1,2,0:T(8,128)}, u32[]{:S(2)}) copy-start(f32[1,512,5120]{1,2,0:T(8,128)} %get-tuple-element.359) | copy-start | bytes 31457284 | tf_op jit(solution)/shard_map/while
  206.3 7.1 %copy-start = (f32[1,512,5120]{1,2,0:T(8,128)S(1)}, f32[1,512,5120]{1,2,0:T(8,128)}, u32[]{:S(2)}) copy-start(f32[1,512,5120]{1,2,0:T(8,128)} %get-tuple-element.359) | copy-start | bytes 31457284 | tf_op jit(solution)/shard_map/while
  238.6 7.0 %copy-start = (f32[1,512,5120]{1,2,0:T(8,128)S(1)}, f32[1,512,5120]{1,2,0:T(8,128)}, u32[]{:S(2)}) copy-start(f32[1,512,5120]{1,2,0:T(8,128)} %get-tuple-element.359) | copy-start | bytes 31457284 | tf_op jit(solution)/shard_map/while
  274.2 7.0 %copy-start = (f32[1,512,5120]{1,2,0:T(8,128)S(1)}, f32[1,512,5120]{1,2,0:T(8,128)}, u32[]{:S(2)}) copy-start(f32[1,512,5120]{1,2,0:T(8,128)} %get-tuple-element.359) | copy-start | bytes 31457284 | tf_op jit(solution)/shard_map/while
  313.0 7.0 %copy-start = (f32[1,512,5120]{1,2,0:T(8,128)S(1)}, f32[1,512,5120]{1,2,0:T(8,128)}, u32[]{:S(2)}) copy-start(f32[1,512,5120]{1,2,0:T(8,128)} %get-tuple-element.359) | copy-start | bytes 31457284 | tf_op jit(solution)/shard_map/while
  355.2 7.0 %copy-start = (f32[1,512,5120]{1,2,0:T(8,128)S(1)}, f32[1,512,5120]{1,2,0:T(8,128)}, u32[]{:S(2)}) copy-start(f32[1,512,5120]{1,2,0:T(8,128)} %get-tuple-element.359) | copy-start | bytes 31457284 | tf_op jit(solution)/shard_map/while
  400.7 7.0 %copy-start = (f32[1,512,5120]{1,2,0:T(8,128)S(1)}, f32[1,512,5120]{1,2,0:T(8,128)}, u32[]{:S(2)}) copy-start(f32[1,512,5120]{1,2,0:T(8,128)} %get-tuple-element.359) | copy-start | bytes 31457284 | tf_op jit(solution)/shard_map/while
  449.4 7.0 %copy-start = (f32[1,512,5120]{1,2,0:T(8,128)S(1)}, f32[1,512,5120]{1,2,0:T(8,128)}, u32[]{:S(2)}) copy-start(f32[1,512,5120]{1,2,0:T(8,128)} %get-tuple-element.359) | copy-start | bytes 31457284 | tf_op jit(solution)/shard_map/while
  501.6 7.0 %copy-start = (f32[1,512,5120]{1,2,0:T(8,128)S(1)}, f32[1,512,5120]{1,2,0:T(8,128)}, u32[]{:S(2)}) copy-start(f32[1,512,5120]{1,2,0:T(8,128)} %get-tuple-element.359) | copy-start | bytes 31457284 | tf_op jit(solution)/shard_map/while
  557.0 7.0 %copy-start = (f32[1,512,5120]{1,2,0:T(8,128)S(1)}, f32[1,512,5120]{1,2,0:T(8,128)}, u32[]{:S(2)}) copy-start(f32[1,512,5120]{1,2,0:T(8,128)} %get-tuple-element.359) | copy-start | bytes 31457284 | tf_op jit(solution)/shard_map/while
  586.7 19.9 %all-to-all-start = ((bf16[16,320,64]{1,2,0:T(8,128)(2,1)}), bf16[16,320,64]{1,2,0:T(8,128)(2,1)S(1)}, u32[]{:S(2)}, u32[]{:S(2)}) async-start(bf16[16,320,64]{1,2,0:T(8,128)(2,1)} %fusion.39), calls=%async_computation | async-start | bytes 1572864 | tf_op jit(solution)/shard_map/all_to_all | solution.py:115
Sparse Core Ops, SparseCore 0:
  9.5 140.5 all-gather.14
  151.7 29.9 all-gather.16
  183.3 30.9 all-gather.18
where the time goes:
time: 623 us; the launch traced here: 617 us
  matrix products  158 us (25%)
  other arithmetic  145 us (23%)
  local copies, waits for them, and re-layouts  124 us (20%)
  blocking collectives  89.7 us (14%)
  waiting for transfers between devices  65 us (10%)
  loops' own time  16 us (3%)
  between operations  13.4 us (2%)
    all_gather x10, blocking collectives, all_blocks(): pieces = lax.all_gather(pieces, axes[k])  89.7 us
    dot_general x55, matrix products, fill(): jnp.einsum('qhd,khd->hqk', query_block, key_block, preferred_element_type...  73.3 us
    dot_general x55, matrix products, gather_values(): jnp.einsum('hqk,khd->qhd', prob_block, value_block, preferred_element_typ...  69 us
    reduce_sum x10, other arithmetic, one_block(): jnp.sum(weights, axis=-1, keepdims=True)  55.7 us
    another operation x20, local copies, waits for them, and re-layouts  53.3 us
    all_gather x1, waiting for transfers between devices, on_device(): whole = lax.all_gather(own_rows, SP, axis=0, tiled=True)  51.4 us
    reduce_max x10, other arithmetic, one_block(): peak = jnp.max(scores, axis=-1, keepdims=True)  47.3 us
    convert_element_type x10, other arithmetic, one_block(): (weights / jnp.sum(weights, axis=-1, keepdims=True)).astype(jnp.bfloat16)  38.4 us
  transfers between devices with their start and end apart: 4, of which 2 were waited for; matrix products, arithmetic and copies ran while one was open for 66% of the time, Pallas kernels for 0%

commit v1 on v0

--- a/solution.py
+++ b/solution.py
@@ -102,7 +102,8 @@
     head_dim = qk_gain.shape[1]
     stacked = jnp.stack((w_query, w_key, w_value))
     columns, out_columns = (spread_gather(stacked, DP, 1), spread_gather(w_output, DP, 1))
-    whole = lax.all_gather(own_rows, SP, axis=0, tiled=True)
+    repeated = jnp.stack([own_rows] * lax.axis_size(SP))
+    whole = jnp.concatenate(lax.all_to_all(repeated, SP, 0, 0), axis=0)
     triple = jnp.einsum("td,kdc->ktc", whole, columns, preferred_element_type=jnp.float32).astype(
         jnp.bfloat16
     )

time: 623 us -> 868 us (1.39)
  blocking collectives: 89.7 us -> 362 us
  waiting for transfers between devices: 65 us -> 11.4 us
  local copies, waits for them, and re-layouts: 124 us -> 140 us
  starting transfers between devices: 5.39 us -> 15.4 us
    all_gather x10, blocking collectives: 89.7 us -> 362 us  [all_blocks(): pieces = lax.all_gather(pieces, axes[k])]
    all_gather x1 -> x0, waiting for transfers between devices: 51.4 us -> none  [on_device(): whole = lax.all_gather(own_rows, SP, axis=0, tiled=True)]
    another operation x20 -> x21, local copies, waits for them, and re-layouts: 53.3 us -> 61.6 us
  transfers between devices with their start and end apart: 4 -> 4, of which waited for: 2 -> 1; matrix products, arithmetic and copies ran while one was open for 66% -> 48% of each run, Pallas kernels for 0% -> 0%
where the time goes in v1:
time: 868 us; the launch traced here: 862 us
  blocking collectives  362 us (42%)
  matrix products  158 us (18%)
  other arithmetic  146 us (17%)
  local copies, waits for them, and re-layouts  140 us (16%)
  loops' own time  15.8 us (2%)
  starting transfers between devices  15.4 us (2%)
  between operations  13.7 us (2%)
  waiting for transfers between devices  11.4 us (1%)
    all_gather x10, blocking collectives, all_blocks(): pieces = lax.all_gather(pieces, axes[k])  362 us
    dot_general x55, matrix products, fill(): jnp.einsum('qhd,khd->hqk', query_block, key_block, preferred_element_type...  73.2 us
    dot_general x55, matrix products, gather_values(): jnp.einsum('hqk,khd->qhd', prob_block, value_block, preferred_element_typ...  69 us
    reduce_sum x10, other arithmetic, one_block(): jnp.sum(weights, axis=-1, keepdims=True)  55.6 us
    another operation x20, local copies, waits for them, and re-layouts  53.3 us
    reduce_max x10, other arithmetic, one_block(): peak = jnp.max(scores, axis=-1, keepdims=True)  47.1 us
    convert_element_type x10, other arithmetic, one_block(): (weights / jnp.sum(weights, axis=-1, keepdims=True)).astype(jnp.bfloat16)  38.4 us
    dynamic_slice x55, local copies, waits for them, and re-layouts, fill(): decay_keys = lax.dynamic_slice_in_dim(decay_rows, key_start, block, 1)  37.5 us
  transfers between devices with their start and end apart: 4, of which 1 were waited for; matrix products, arithmetic and copies ran while one was open for 48% of the time, Pallas kernels for 0%

profile of v1, /device:TPU:0, one launch (start us, length us, event | category | flops | bytes accessed | tf_op | source)
XLA Modules:
  0.0 862.1 jit_solution(8069791129823999420)
XLA Ops:
  6.5 8.3 stack.19
  14.8 8.3 all-to-all-start
  23.2 12.2 %all-gather.4 = bf16[128,256]{1,0:T(8,128)(2,1)S(1)} all-gather(bf16[32,256]{1,0:T(8,128)(2,1)S(1)} %get-tuple-element.211), channel_id=6, replica_groups=mesh['sp_0'=4,'sp_1'=4,'dp_0'=4,'dp_1'=2] {'dp_0'}, dimensions={0}, use_global_device_ids=true | all-gather | bytes 81920 | tf_op jit(solution)/shard_map/all_gather | solution.py:21
  39.2 12.0 %all-gather.7 = bf16[8,32,256]{2,1,0:T(8,128)(2,1)S(1)} all-gather(bf16[2,32,256]{2,1,0:T(8,128)(2,1)S(1)} %bitcast.141), channel_id=9, replica_groups=mesh['sp_0'=4,'sp_1'=4,'dp_0'=4,'dp_1'=2] {'dp_0'}, dimensions={0}, use_global_device_ids=true | all-gather | bytes 163840 | tf_op jit(solution)/shard_map/all_gather | solution.py:21
  51.4 228.1 %all_gather.89 = bf16[4,32,2048]{2,1,0:T(8,128)(2,1)} all-gather(bf16[1,32,2048]{2,1,0:T(8,128)(2,1)S(1)} %all_gather.88), channel_id=1, replica_groups=mesh['sp_0'=4,'sp_1'=4,'dp_0'=4,'dp_1'=2] {'sp_0'}, dimensions={0}, use_global_device_ids=true | all-gather | bytes 655360 | tf_op jit(solution)/shard_map/all_gather | solution.py:21
  279.7 76.9 %all_gather.93 = bf16[4,32,2048]{2,1,0:T(8,128)(2,1)} all-gather(bf16[1,32,2048]{2,1,0:T(8,128)(2,1)S(1)} %all_gather.92), channel_id=1, replica_groups=mesh['sp_0'=4,'sp_1'=4,'dp_0'=4,'dp_1'=2] {'sp_1'}, dimensions={0}, use_global_device_ids=true | all-gather | bytes 655360 | tf_op jit(solution)/shard_map/all_gather | solution.py:21
  356.7 12.5 %all-gather = bf16[12,128,64]{1,2,0:T(8,128)(2,1)S(1)} all-gather(bf16[3,128,64]{1,2,0:T(8,128)(2,1)S(1)} %get-tuple-element.209), channel_id=2, replica_groups=mesh['sp_0'=4,'sp_1'=4,'dp_0'=4,'dp_1'=2] {'dp_0'}, dimensions={0}, use_global_device_ids=true | all-gather | bytes 245760 | tf_op jit(solution)/shard_map/all_gather | solution.py:21
  373.1 12.5 %all-gather.3 = bf16[8,3,128,64]{2,3,1,0:T(8,128)(2,1)S(1)} all-gather(bf16[2,3,128,64]{2,3,1,0:T(8,128)(2,1)S(1)} %bitcast.138), channel_id=5, replica_groups=mesh['sp_0'=4,'sp_1'=4,'dp_0'=4,'dp_1'=2] {'dp_0'}, dimensions={0}, use_global_device_ids=true | all-gather | bytes 491520 | tf_op jit(solution)/shard_map/all_gather | solution.py:21
  385.9 11.4 %fusion.18 = bf16[3,5120,64]{1,2,0:T(8,128)(2,1)S(1)} fusion(bf16[3,2048,64]{1,2,0:T(8,128)(2,1)S(1)} %bitcast.134, bf16[5120,2048,1]{1,0,2:T(8,128)(2,1)} %bitcast.18), kind=kOutput, calls=%fused_computation.28 | convolution fusion | flops 4027514880 | bytes 23724032 | tf_op jit(solution)/shard_map/td,kdc->ktc/dot_general | solution.py:107
  398.1 424.4 %while.33 = (s32[]{:T(128)}, f32[10,512,1,64]{1,3,2,0:T(8,128)}, s32[10]{0:T(128)S(1)}, bf16[5120,1,64]{0,2,1:T(8,128)(2,1)S(1)}, f32[1,5120]{1,0:T(1,128)}, /*i...) while((s32[]{:T(128)}, f32[10,512,1,64]{1,3,2,0:T(8,128)}, ...), condition=%wide.region_9.10_spmd, body=%wide.region_2.9_spmd.sunk | while | flops 83918864 | bytes 91718952 | solution.py:94
  412.9 5.6 fusion.54
  442.5 5.6 fusion.54
  464.6 6.0 while.34
  498.8 8.1 while.34
  511.5 5.6 fusion.54
  536.2 10.1 %while.34 = (s32[]{:T(128)}, f32[1,512,5120]{1,2,0:T(8,128)}, s32[]{:T(128)}, bf16[5120,1,64]{0,2,1:T(8,128)(2,1)S(1)}, bf16[512,1,64]{0,2,1:T(8,128)(2,1)S(1)},...) while((s32[]{:T(128)}, f32[1,512,5120]{1,2,0:T(8,128)}, ...), condition=%wide.region_4.4_spmd.clone, body=%wide.region_3.3_spmd.clone.sunk | while | flops 34604036 | bytes 1197231 | solution.py:78
  551.0 5.6 fusion.54
  561.8 6.4 while.35
  577.0 12.1 %while.34 = (s32[]{:T(128)}, f32[1,512,5120]{1,2,0:T(8,128)}, s32[]{:T(128)}, bf16[5120,1,64]{0,2,1:T(8,128)(2,1)S(1)}, bf16[512,1,64]{0,2,1:T(8,128)(2,1)S(1)},...) while((s32[]{:T(128)}, f32[1,512,5120]{1,2,0:T(8,128)}, ...), condition=%wide.region_4.4_spmd.clone, body=%wide.region_3.3_spmd.clone.sunk | while | flops 34604036 | bytes 1197231 | solution.py:78
  593.8 5.6 fusion.54
  604.6 7.7 while.35
  621.1 14.1 %while.34 = (s32[]{:T(128)}, f32[1,512,5120]{1,2,0:T(8,128)}, s32[]{:T(128)}, bf16[5120,1,64]{0,2,1:T(8,128)(2,1)S(1)}, bf16[512,1,64]{0,2,1:T(8,128)(2,1)S(1)},...) while((s32[]{:T(128)}, f32[1,512,5120]{1,2,0:T(8,128)}, ...), condition=%wide.region_4.4_spmd.clone, body=%wide.region_3.3_spmd.clone.sunk | while | flops 34604036 | bytes 1197231 | solution.py:78
  639.9 5.6 fusion.54
  650.7 9.0 %while.35 = (s32[]{:T(128)}, f32[512,1,64]{0,2,1:T(8,128)S(1)}, s32[]{:T(128)}, bf16[5120,1,64]{0,2,1:T(8,128)(2,1)S(1)}, bf16[1,512,5120]{1,2,0:T(8,128)(2,1)},...) while((s32[]{:T(128)}, f32[512,1,64]{0,2,1:T(8,128)S(1)}, s32[]{:T(128)}, ...), condition=%wide.region_8.8_spmd, body=%wide.region_7.7_spmd.sunk | while | flops 33587204 | bytes 853131 | solution.py:92
  668.4 16.1 %while.34 = (s32[]{:T(128)}, f32[1,512,5120]{1,2,0:T(8,128)}, s32[]{:T(128)}, bf16[5120,1,64]{0,2,1:T(8,128)(2,1)S(1)}, bf16[512,1,64]{0,2,1:T(8,128)(2,1)S(1)},...) while((s32[]{:T(128)}, f32[1,512,5120]{1,2,0:T(8,128)}, ...), condition=%wide.region_4.4_spmd.clone, body=%wide.region_3.3_spmd.clone.sunk | while | flops 34604036 | bytes 1197231 | solution.py:78
  700.1 10.3 %while.35 = (s32[]{:T(128)}, f32[512,1,64]{0,2,1:T(8,128)S(1)}, s32[]{:T(128)}, bf16[5120,1,64]{0,2,1:T(8,128)(2,1)S(1)}, bf16[1,512,5120]{1,2,0:T(8,128)(2,1)},...) while((s32[]{:T(128)}, f32[512,1,64]{0,2,1:T(8,128)S(1)}, s32[]{:T(128)}, ...), condition=%wide.region_8.8_spmd, body=%wide.region_7.7_spmd.sunk | while | flops 33587204 | bytes 853131 | solution.py:92
  719.1 18.2 %while.34 = (s32[]{:T(128)}, f32[1,512,5120]{1,2,0:T(8,128)}, s32[]{:T(128)}, bf16[5120,1,64]{0,2,1:T(8,128)(2,1)S(1)}, bf16[512,1,64]{0,2,1:T(8,128)(2,1)S(1)},...) while((s32[]{:T(128)}, f32[1,512,5120]{1,2,0:T(8,128)}, ...), condition=%wide.region_4.4_spmd.clone, body=%wide.region_3.3_spmd.clone.sunk | while | flops 34604036 | bytes 1197231 | solution.py:78
  752.9 11.6 %while.35 = (s32[]{:T(128)}, f32[512,1,64]{0,2,1:T(8,128)S(1)}, s32[]{:T(128)}, bf16[5120,1,64]{0,2,1:T(8,128)(2,1)S(1)}, bf16[1,512,5120]{1,2,0:T(8,128)(2,1)},...) while((s32[]{:T(128)}, f32[512,1,64]{0,2,1:T(8,128)S(1)}, s32[]{:T(128)}, ...), condition=%wide.region_8.8_spmd, body=%wide.region_7.7_spmd.sunk | while | flops 33587204 | bytes 853131 | solution.py:92
  773.2 20.2 %while.34 = (s32[]{:T(128)}, f32[1,512,5120]{1,2,0:T(8,128)}, s32[]{:T(128)}, bf16[5120,1,64]{0,2,1:T(8,128)(2,1)S(1)}, bf16[512,1,64]{0,2,1:T(8,128)(2,1)S(1)},...) while((s32[]{:T(128)}, f32[1,512,5120]{1,2,0:T(8,128)}, ...), condition=%wide.region_4.4_spmd.clone, body=%wide.region_3.3_spmd.clone.sunk | while | flops 34604036 | bytes 1197231 | solution.py:78
  808.9 12.9 %while.35 = (s32[]{:T(128)}, f32[512,1,64]{0,2,1:T(8,128)S(1)}, s32[]{:T(128)}, bf16[5120,1,64]{0,2,1:T(8,128)(2,1)S(1)}, bf16[1,512,5120]{1,2,0:T(8,128)(2,1)},...) while((s32[]{:T(128)}, f32[512,1,64]{0,2,1:T(8,128)S(1)}, s32[]{:T(128)}, ...), condition=%wide.region_8.8_spmd, body=%wide.region_7.7_spmd.sunk | while | flops 33587204 | bytes 853131 | solution.py:92
  831.1 7.0 all-to-all-start.1
  839.8 11.3 %all-to-all-done.1 = bf16[16,320,64]{1,2,0:T(8,128)(2,1)S(1)} async-done(((bf16[16,320,64]{1,2,0:T(8,128)(2,1)}), bf16[16,320,64]{1,2,0:T(8,128)(2,1)S(1)}, u32[]{:S(2)}, u32[]{:S(2)}) %all-to-all-start.1) | async-done | bytes 655392 | tf_op jit(solution)/shard_map/all_to_all | solution.py:116
  (379 shorter events, 417.8 us)
Async XLA Ops:
  14.8 8.4 copy-start.1
  14.8 371.1 %all-to-all-start = ((bf16[16,320,2048]{2,1,0:T(8,128)(2,1)}), bf16[16,320,2048]{2,1,0:T(8,128)(2,1)}, u32[]{:S(2)}, u32[]{:S(2)}) async-start(bf16[16,320,2048]{2,1,0:T(8,128)(2,1)} %stack.19), calls=%async_computation | async-start | bytes 41943040 | tf_op jit(solution)/shard_map/all_to_all | solution.py:106
  23.1 814.9 %all-gather.13.cloned.1.call-start = ((), (), s32[]{:S(2)}) async-start(), calls=%async_computation.2 | async-start | bytes 2621440 | tf_op jit(solution)/shard_map/all_gather | solution.py:21
  51.2 305.4 %copy-start.2 = (bf16[256,64]{0,1:T(8,128)(2,1)S(1)}, bf16[256,64]{0,1:T(8,128)(2,1)}, u32[]{:S(2)}) copy-start(bf16[256,64]{0,1:T(8,128)(2,1)} %param.16) | copy-start | bytes 98308
  51.2 305.4 %copy-start.3 = (bf16[256,64]{0,1:T(8,128)(2,1)S(1)}, bf16[256,64]{0,1:T(8,128)(2,1)}, u32[]{:S(2)}) copy-start(bf16[256,64]{0,1:T(8,128)(2,1)} %param.15) | copy-start | bytes 98308
  51.2 305.4 %copy-start.4 = (bf16[256,64]{0,1:T(8,128)(2,1)S(1)}, bf16[256,64]{0,1:T(8,128)(2,1)}, u32[]{:S(2)}) copy-start(bf16[256,64]{0,1:T(8,128)(2,1)} %param.14) | copy-start | bytes 98308
  279.5 560.3 %all-gather.15.cloned.1.call-start = ((), (), s32[]{:S(2)}) async-start(), calls=%async_computation.3 | async-start | bytes 2621440 | tf_op jit(solution)/shard_map/all_gather | solution.py:21
  371.2 14.6 %copy-start.5 = (f32[2,64]{1,0:T(2,128)S(1)}, f32[2,64]{1,0:T(2,128)}, u32[]{:S(2)}) copy-start(f32[2,64]{1,0:T(2,128)} %param.18) | copy-start | bytes 1540
  412.9 7.0 copy-start
  442.5 7.0 copy-start
  475.4 7.0 copy-start
  511.5 7.0 copy-start
  551.0 7.0 copy-start
  593.8 7.0 copy-start
  639.9 7.0 copy-start
  689.3 7.0 copy-start
  742.1 7.0 copy-start
  798.1 7.0 copy-start
  831.1 20.0 %all-to-all-start.1 = ((bf16[16,320,64]{1,2,0:T(8,128)(2,1)}), bf16[16,320,64]{1,2,0:T(8,128)(2,1)S(1)}, u32[]{:S(2)}, u32[]{:S(2)}) async-start(bf16[16,320,64]{1,2,0:T(8,128)(2,1)} %fusion.32), calls=%async_computation.1 | async-start | bytes 1572864 | tf_op jit(solution)/shard_map/all_to_all | solution.py:116
Sparse Core Ops, SparseCore 0:
  279.6 72.8 all-gather.12
  356.7 32.2 all-gather.14
